TPU v7x, 32 devices: a whole 2x2x4 slice. The times are simulated.
32 devices in a mesh: fs: 8 (over z, y), tp: 4 (over x, core).
Axes of the slice: x: 2, y: 2, z: 4, core: 2. Of those that a mesh axis runs over, the one named last changes fastest.
Arguments:
- later_input: bfloat16 [4096, 2048], P(('fs', 'tp')), may hold values from -6 to 6
- earlier_input: bfloat16 [4096, 2048], P('fs'), may hold values from -6 to 6
- earlier_hidden: bfloat16 [4096, 4096], P('fs', 'tp'), may hold values from -6 to 6
- cotangent: bfloat16 [4096, 2048], P('fs'), may hold values from -6 to 6
- up_weight: bfloat16 [2048, 4096], P('fs', 'tp'), may hold values from -0.125 to 0.125
- down_weight: bfloat16 [4096, 2048], P(('tp', 'fs')), may hold values from -0.09375 to 0.09375
- up_sum: float32 [2048, 4096], P('fs', 'tp'), may hold values from -4 to 4
- down_sum: float32 [4096, 2048], P(('tp', 'fs')), may hold values from -4 to 4
Outputs:
- later_output: bfloat16 [4096, 2048], P(('fs', 'tp'))
- later_hidden: bfloat16 [4096, 4096], P('fs', 'tp')
- earlier_grad: bfloat16 [4096, 2048], P(('fs', 'tp'))
- up_sum_next: float32 [2048, 4096], P('fs', 'tp')
- down_sum_next: float32 [4096, 2048], P(('tp', 'fs'))
All inputs are finite; a program needn't handle non-finite values.
Results may differ from a plain program's by a relative error of at most 0.0095.
Values may be sent and summed in bfloat16 or wider, within the bound.
A program may use at most 128 MiB of HBM per device.

v0:
```python
import jax
import jax.numpy as jnp
from jax import lax
from jax.sharding import PartitionSpec as P


def contract_last(left_rows, right_rows):
    return lax.dot_general(
        left_rows, right_rows, (((1,), (1,)), ((), ())), preferred_element_type=jnp.float32
    )


def contract_first(left_rows, right_rows):
    return lax.dot_general(
        left_rows, right_rows, (((0,), (0,)), ((), ())), preferred_element_type=jnp.float32
    )


def shards(
    later_input, earlier_input, earlier_hidden, cotangent, up_weight, down_weight, up_sum, down_sum
):
    gathered = lax.all_gather(later_input, "tp", axis=0, tiled=True)
    groups = lax.axis_size("fs")
    grad_scale = float(earlier_input.shape[0] * groups) ** (-0.5)
    lifted = jnp.maximum(earlier_hidden.astype(jnp.float32), 0.0)
    activation = (lifted * lifted).astype(jnp.bfloat16)
    up_front, down_front = (
        lax.all_gather(up_weight, "fs", axis=0, tiled=True),
        lax.all_gather(down_weight, "fs", axis=0, tiled=True),
    )
    later_hidden = jnp.dot(gathered, up_front, preferred_element_type=jnp.float32).astype(
        jnp.bfloat16
    )
    lifted_later = jnp.maximum(later_hidden.astype(jnp.float32), 0.0)
    act_later = (lifted_later * lifted_later).astype(jnp.bfloat16)
    rows_here = act_later
    later_output = lax.psum_scatter(
        jnp.dot(rows_here, down_front, preferred_element_type=jnp.float32).astype(jnp.bfloat16),
        "tp",
        scatter_dimension=0,
        tiled=True,
    )
    up_back, down_back = (up_front, down_front)
    act_slope = contract_last(cotangent, down_back)
    pre_grad = (2.0 * act_slope * lifted).astype(jnp.bfloat16)
    rows_here = pre_grad
    earlier_grad = lax.psum_scatter(
        contract_last(rows_here, up_back).astype(jnp.bfloat16),
        "tp",
        scatter_dimension=0,
        tiled=True,
    )
    columns = earlier_input
    up_total = lax.psum_scatter(
        contract_first(columns, pre_grad), "fs", scatter_dimension=0, tiled=True
    )
    earlier_grad, up_total = (earlier_grad, up_total)
    columns = activation
    down_total = lax.psum_scatter(
        contract_first(columns, cotangent), "fs", scatter_dimension=0, tiled=True
    )
    return (
        later_output,
        later_hidden,
        earlier_grad,
        up_sum + grad_scale * up_total,
        down_sum + grad_scale * down_total,
    )


def solution(mesh):
    in_specs = (
        P(("fs", "tp"), None),
        P("fs", None),
        P("fs", "tp"),
        P("fs", None),
        P("fs", "tp"),
        P(("tp", "fs"), None),
        P("fs", "tp"),
        P(("tp", "fs"), None),
    )
    out_specs = (
        P(("fs", "tp"), None),
        P("fs", "tp"),
        P(("fs", "tp"), None),
        P("fs", "tp"),
        P(("tp", "fs"), None),
    )
    return jax.shard_map(shards, mesh=mesh, in_specs=in_specs, out_specs=out_specs, check_vma=False)
```

profile of v0, /device:TPU:0, one launch (start us, length us, event | category | flops | bytes accessed | tf_op | source)
XLA Modules:
  0.0 557.7 jit_solution(5843369301261905202)
XLA Ops:
  7.2 0.0 all-gather.8.cloned.1.call-start
  7.2 0.7 all-gather.8.cloned.1.call-update
  7.9 0.0 all-gather.6.cloned.1.call-start
  8.0 0.7 all-gather.6.cloned.1.call-update
  8.7 0.0 all-gather.4.cloned.1.call-start
  8.7 0.7 all-gather.4.cloned.1.call-update
  9.4 0.0 reduce-scatter.11.cloned.1.call-start
  9.5 6.9 %fusion = f32[1024,2048]{1,0:T(8,128)} fusion(bf16[512,2048]{1,0:T(8,128)(2,1)S(1)} %copy-done, bf16[512,1024]{1,0:T(8,128)(2,1)} %param.10), kind=kOutput, calls=%fused_computation.8 | convolution fusion | flops 2149580800 | bytes 11534336 | tf_op jit(solution)/shard_map/dot_general | solution.py:14
  16.3 0.0 reduce-scatter.11.cloned.1.call-update
  16.3 0.0 reduce-scatter.9.cloned.1.call-start
  16.4 69.3 %all-gather.8.cloned.1.call-done = bf16[1024,2048]{1,0:T(8,128)(2,1)} async-done(((bf16[128,2048]{1,0:T(8,128)(2,1)}), bf16[1024,2048]{1,0:T(8,128)(2,1)}) %all-gather.8.cloned.1.call-update) | async-done | bytes 4194320 | tf_op jit(solution)/shard_map/all_gather | solution.py:29
  85.7 4.7 multiply_convert_fusion.1
  90.4 1.0 copy-done.5
  91.4 5.6 %convolution_bitcast_fusion = f32[2048,1024]{0,1:T(8,128)} fusion(bf16[512,1024]{1,0:T(8,128)(2,1)S(1)} %multiply_convert_fusion.1, bf16[512,2048]{1,0:T(8,128)(2,1)S(1)} %copy-done.2), kind=kOutput, calls=%fused_computation | convolution fusion | flops 2147483648 | bytes 11534336 | tf_op jit(solution)/shard_map/dot_general | solution.py:14
  97.0 0.0 reduce-scatter.9.cloned.1.call-update
  97.0 0.0 reduce-scatter.7.cloned.1.call-start
  97.1 62.1 %all-gather.6.cloned.1.call-done = bf16[2048,1024]{1,0:T(8,128)(2,1)} async-done(((bf16[256,1024]{1,0:T(8,128)(2,1)}), bf16[2048,1024]{1,0:T(8,128)(2,1)}) %all-gather.6.cloned.1.call-update) | async-done | bytes 4194320 | tf_op jit(solution)/shard_map/all_gather | solution.py:28
  159.1 5.9 %convolution_convert_fusion = bf16[512,2048]{1,0:T(8,128)(2,1)} fusion(bf16[512,1024]{1,0:T(8,128)(2,1)S(1)} %copy-done.6, bf16[2048,1024]{1,0:T(8,128)(2,1)} %all-gather.6.cloned.1.call-done), kind=kOutput, calls=%fused_computation.1 | convolution fusion | flops 2148532224 | bytes 7340032 | tf_op jit(solution)/shard_map/dot_general | solution.py:8
  165.1 0.0 reduce-scatter.7.cloned.1.call-update
  165.1 0.2 reduce-scatter.5.cloned.1.call-start
  165.3 16.5 %all-gather.4.cloned.1.call-done = bf16[512,2048]{1,0:T(8,128)(2,1)} async-done(((bf16[128,2048]{1,0:T(8,128)(2,1)}), bf16[512,2048]{1,0:T(8,128)(2,1)}) %all-gather.4.cloned.1.call-update) | async-done | bytes 2097168 | tf_op jit(solution)/shard_map/all_gather | solution.py:22
  181.8 5.3 convolution_convert_fusion.2
  187.2 1.0 copy-done.4
  188.1 3.7 convolution_convert_fusion.1
  191.8 1.9 copy.13
  193.7 139.1 %reduce-scatter.11.cloned.1.call-done = f32[128,2048]{1,0:T(8,128)} async-done(((f32[1024,2048]{1,0:T(8,128)}), f32[128,2048]{1,0:T(8,128)}) %reduce-scatter.11.cloned.1.call-update) | async-done | bytes 1048592 | tf_op jit(solution)/shard_map/reduce_scatter | solution.py:59
  332.8 2.6 multiply_add_fusion
  335.5 147.8 %reduce-scatter.9.cloned.1.call-done = f32[256,1024]{0,1:T(8,128)} async-done(((f32[2048,1024]{0,1:T(8,128)}), f32[256,1024]{0,1:T(8,128)}) %reduce-scatter.9.cloned.1.call-update) | async-done | bytes 1048592 | tf_op jit(solution)/shard_map/reduce_scatter | solution.py:54
  483.3 2.3 multiply_add_fusion.1
  485.6 2.5 copy.14
  488.2 28.4 %reduce-scatter.7.cloned.1.call-done = bf16[128,2048]{1,0:T(8,128)(2,1)} async-done(((bf16[512,2048]{1,0:T(8,128)(2,1)}), bf16[128,2048]{1,0:T(8,128)(2,1)}) %reduce-scatter.7.cloned.1.call-update) | async-done | bytes 524304 | tf_op jit(solution)/shard_map/reduce_scatter | solution.py:47
  516.6 34.3 %reduce-scatter.5.cloned.1.call-done = bf16[128,2048]{1,0:T(8,128)(2,1)} async-done(((bf16[512,2048]{1,0:T(8,128)(2,1)}), bf16[128,2048]{1,0:T(8,128)(2,1)}) %reduce-scatter.5.cloned.1.call-update) | async-done | bytes 524304 | tf_op jit(solution)/shard_map/reduce_scatter | solution.py:37
  (13 shorter events, 0.0 us)
Async XLA Ops:
  7.2 2.3 copy-start
  7.2 78.5 %all-gather.8.cloned.1.call-start = ((), (), s32[]{:S(2)}) async-start(), calls=%async_computation.6 | async-start | bytes 4718592 | tf_op jit(solution)/shard_map/all_gather | solution.py:29
  7.9 151.2 %all-gather.6.cloned.1.call-start = ((), (), s32[]{:S(2)}) async-start(), calls=%async_computation.5 | async-start | bytes 4718592 | tf_op jit(solution)/shard_map/all_gather | solution.py:28
  8.7 173.2 %all-gather.4.cloned.1.call-start = ((), (), s32[]{:S(2)}) async-start(), calls=%async_computation.4 | async-start | bytes 2621440 | tf_op jit(solution)/shard_map/all_gather | solution.py:22
  9.4 323.4 %reduce-scatter.11.cloned.1.call-start = ((), (), s32[]{:S(2)}) async-start(), calls=%async_computation.10 | async-start | bytes 9437184 | tf_op jit(solution)/shard_map/reduce_scatter | solution.py:59
  16.3 69.3 %copy-start.3 = (bf16[512,1024]{1,0:T(8,128)(2,1)S(1)}, bf16[512,1024]{1,0:T(8,128)(2,1)}, u32[]{:S(2)}) copy-start(bf16[512,1024]{1,0:T(8,128)(2,1)} %param.10) | copy-start | bytes 3145732
  16.3 467.0 %reduce-scatter.9.cloned.1.call-start = ((), (), s32[]{:S(2)}) async-start(), calls=%async_computation.9 | async-start | bytes 9437184 | tf_op jit(solution)/shard_map/reduce_scatter | solution.py:54
  85.7 5.7 %copy-start.2 = (bf16[512,2048]{1,0:T(8,128)(2,1)S(1)}, bf16[512,2048]{1,0:T(8,128)(2,1)}, u32[]{:S(2)}) copy-start(bf16[512,2048]{1,0:T(8,128)(2,1)} %param.9) | copy-start | bytes 6291460
  90.4 1.0 copy-start.5
  97.0 62.2 %copy-start.6 = (bf16[512,1024]{1,0:T(8,128)(2,1)S(1)}, bf16[512,1024]{1,0:T(8,128)(2,1)}, u32[]{:S(2)}) copy-start(bf16[512,1024]{1,0:T(8,128)(2,1)} %copy-done.5) | copy-start | bytes 3145732
  97.0 419.6 %reduce-scatter.7.cloned.1.call-start = ((), (), s32[]{:S(2)}) async-start(), calls=%async_computation.8 | async-start | bytes 2621440 | tf_op jit(solution)/shard_map/reduce_scatter | solution.py:47
  165.1 385.8 %reduce-scatter.5.cloned.1.call-start = ((), (), s32[]{:S(2)}) async-start(), calls=%async_computation.7 | async-start | bytes 2621440 | tf_op jit(solution)/shard_map/reduce_scatter | solution.py:37
  181.8 6.3 %copy-start.1 = (bf16[1024,2048]{1,0:T(8,128)(2,1)S(1)}, bf16[1024,2048]{1,0:T(8,128)(2,1)}, u32[]{:S(2)}) copy-start(bf16[1024,2048]{1,0:T(8,128)(2,1)} %all-gather.8.cloned.1.call-done) | copy-start | bytes 12582916
  187.1 1.0 copy-start.4
Sparse Core Ops, SparseCore 0:
  10.1 75.5 all-gather.7
  87.8 71.3 all-gather.5
  160.7 21.0 all-gather.3
  185.3 147.4 reduce-scatter.10
  336.3 146.9 reduce-scatter.8
  486.3 30.2 reduce-scatter.6
  519.7 31.1 reduce-scatter.4
where the time goes:
time: 558 us
  waiting for transfers between devices  500 us (90%)
  matrix products  32.1 us (6%)
  between operations  14.2 us (3%)
  local copies, waits for them, and re-layouts  6.36 us (1%)
    reduce_scatter x1, waiting for transfers between devices, shards(): lax.psum_scatter(contract_first(columns, pre_grad), 'fs', scatter_dimensi...  148 us
    reduce_scatter x1, waiting for transfers between devices, shards(): lax.psum_scatter(contract_first(columns, cotangent), 'fs', scatter_dimens...  139 us
    all_gather x1, waiting for transfers between devices, shards(): lax.all_gather(down_weight, 'fs', axis=0, tiled=True)  69.3 us
    all_gather x1, waiting for transfers between devices, shards(): lax.all_gather(up_weight, 'fs', axis=0, tiled=True)  62.1 us
    reduce_scatter x1, waiting for transfers between devices, shards(): lax.psum_scatter(jnp.dot(rows_here, down_front, preferred_element_type=jn...  34.3 us
    reduce_scatter x1, waiting for transfers between devices, shards(): lax.psum_scatter(contract_last(rows_here, up_back).astype(jnp.bfloat16),...  28.4 us
    all_gather x1, waiting for transfers between devices, shards(): gathered = lax.all_gather(later_input, 'tp', axis=0, tiled=True)  16.5 us
    dot_general x2, matrix products, contract_first(): lax.dot_general(left_rows, right_rows, (((0,), (0,)), ((), ())), preferre...  12.5 us
  transfers between devices with their start and end apart: 7, of which 7 were waited for; matrix products, arithmetic and copies ran while one was open for 7% of the time, Pallas kernels for 0%

commit v1 on v0

--- a/solution.py
+++ b/solution.py
@@ -1,7 +1,28 @@
+import functools
 import jax
 import jax.numpy as jnp
 from jax import lax
 from jax.sharding import PartitionSpec as P
+
+
+def open_the_ratios(point, pos_dim):
+    built = lax.axis_index("fs")
+    o_now = lax.axis_size("fs")
+    lower, v_next, block_now = (o_now, built, point.shape[pos_dim])
+    y1 = jnp.zeros(
+        (*point.shape[:pos_dim], lower * block_now, *point.shape[pos_dim + 1 :]), point.dtype
+    )
+    extra = point
+    trail = [(i0, (i0 + 1) % lower) for i0 in range(lower)]
+    for q in tuple(range(lower)):
+        inter = (v_next - q) % lower
+        y1 = lax.dynamic_update_slice_in_dim(y1, extra, inter * block_now, axis=pos_dim)
+        if q < lower - 1:
+            extra = lax.ppermute(extra, "fs", trail)
+    return y1
+
+
+plan_columns = functools.partial(open_the_ratios, pos_dim=0)
 
 
 def contract_last(left_rows, right_rows):
@@ -26,7 +47,7 @@
     activation = (lifted * lifted).astype(jnp.bfloat16)
     up_front, down_front = (
         lax.all_gather(up_weight, "fs", axis=0, tiled=True),
-        lax.all_gather(down_weight, "fs", axis=0, tiled=True),
+        plan_columns(down_weight),
     )
     later_hidden = jnp.dot(gathered, up_front, preferred_element_type=jnp.float32).astype(
         jnp.bfloat16

time: 558 us -> 524 us (0.939)
  waiting for transfers between devices: 500 us -> 460 us
    ppermute x0 -> x7, waiting for transfers between devices: none -> 147 us  [open_the_ratios(): extra = lax.ppermute(extra, 'fs', trail)]
    all_gather x1 -> x0, waiting for transfers between devices: 69.3 us -> none  [shards(): lax.all_gather(down_weight, 'fs', axis=0, tiled=True)]
    all_gather x1, waiting for transfers between devices: 62.1 us -> 0.02 us  [shards(): lax.all_gather(up_weight, 'fs', axis=0, tiled=True)]
    reduce_scatter x1, waiting for transfers between devices: 139 us -> 101 us  [shards(): lax.psum_scatter(contract_first(columns, cotangent), 'fs', scatter_dimens...]
    all_gather x1, waiting for transfers between devices: 16.5 us -> 0.02 us  [shards(): gathered = lax.all_gather(later_input, 'tp', axis=0, tiled=True)]
    reduce_scatter x1, waiting for transfers between devices: 34.3 us -> 28.3 us  [shards(): lax.psum_scatter(jnp.dot(rows_here, down_front, preferred_element_type=jn...]
    reduce_scatter x1, waiting for transfers between devices: 28.4 us -> 34.2 us  [shards(): lax.psum_scatter(contract_last(rows_here, up_back).astype(jnp.bfloat16),...]
  transfers between devices with their start and end apart: 7 -> 13, of which waited for: 7 -> 11; matrix products, arithmetic and copies ran while one was open for 7% -> 8% of each run, Pallas kernels for 0% -> 0%
where the time goes in v1:
time: 524 us
  waiting for transfers between devices  460 us (88%)
  matrix products  29.9 us (6%)
  between operations  14.3 us (3%)
  local copies, waits for them, and re-layouts  11.4 us (2%)
    reduce_scatter x1, waiting for transfers between devices, shards(): lax.psum_scatter(contract_first(columns, pre_grad), 'fs', scatter_dimensi...  148 us
    ppermute x7, waiting for transfers between devices, open_the_ratios(): extra = lax.ppermute(extra, 'fs', trail)  147 us
    reduce_scatter x1, waiting for transfers between devices, shards(): lax.psum_scatter(contract_first(columns, cotangent), 'fs', scatter_dimens...  101 us
    reduce_scatter x1, waiting for transfers between devices, shards(): lax.psum_scatter(contract_last(rows_here, up_back).astype(jnp.bfloat16),...  34.2 us
    reduce_scatter x1, waiting for transfers between devices, shards(): lax.psum_scatter(jnp.dot(rows_here, down_front, preferred_element_type=jn...  28.3 us
    dot_general x2, matrix products, contract_first(): lax.dot_general(left_rows, right_rows, (((0,), (0,)), ((), ())), preferre...  12.5 us
  transfers between devices with their start and end apart: 13, of which 11 were waited for; matrix products, arithmetic and copies ran while one was open for 8% of the time, Pallas kernels for 0%

profile of v1, /device:TPU:0, one launch (start us, length us, event | category | flops | bytes accessed | tf_op | source)
XLA Modules:
  0.0 523.6 jit_solution(11652913300027718504)
XLA Ops:
  7.2 0.7 all-gather.3.cloned.1.call-update
  8.0 0.7 all-gather.5.cloned.1.call-update
  8.8 6.9 %fusion.1 = f32[1024,2048]{1,0:T(8,128)} fusion(bf16[512,2048]{1,0:T(8,128)(2,1)S(1)} %copy-done, bf16[512,1024]{1,0:T(8,128)(2,1)} %param.10), kind=kOutput, calls=%fused_computation.9 | convolution fusion | flops 2149580800 | bytes 11534336 | tf_op jit(solution)/shard_map/dot_general | solution.py:35
  15.7 1.0 copy-done.3
  16.7 3.0 collective-permute-start
  19.7 15.0 %collective-permute-done = bf16[128,2048]{1,0:T(8,128)(2,1)S(1)} collective-permute-done((bf16[128,2048]{1,0:T(8,128)(2,1)S(1)}, bf16[128,2048]{1,0:T(8,128)(2,1)S(1)}, u32[]{:S(2)}, u32[]{:S(2)}) %collective-permute-start) | collective-permute-done | bytes 524320 | tf_op jit(solution)/shard_map/ppermute | solution.py:21
  34.6 15.9 %collective-permute-done.1 = bf16[128,2048]{1,0:T(8,128)(2,1)S(1)} collective-permute-done((bf16[128,2048]{1,0:T(8,128)(2,1)S(1)}, bf16[128,2048]{1,0:T(8,128)(2,1)S(1)}, u32[]{:S(2)}, u32[]{:S(2)}) %collective-permute-start.1) | collective-permute-done | bytes 524320 | tf_op jit(solution)/shard_map/ppermute | solution.py:21
  50.5 0.8 copy-done.4
  51.3 27.6 %collective-permute-done.2 = bf16[128,2048]{1,0:T(8,128)(2,1)S(1)} collective-permute-done((bf16[128,2048]{1,0:T(8,128)(2,1)S(1)}, bf16[128,2048]{1,0:T(8,128)(2,1)S(1)}, u32[]{:S(2)}, u32[]{:S(2)}) %collective-permute-start.2) | collective-permute-done | bytes 524320 | tf_op jit(solution)/shard_map/ppermute | solution.py:21
  78.9 0.8 copy-done.6
  79.7 26.2 %collective-permute-done.3 = bf16[128,2048]{1,0:T(8,128)(2,1)} collective-permute-done((bf16[128,2048]{1,0:T(8,128)(2,1)S(1)}, bf16[128,2048]{1,0:T(8,128)(2,1)}, u32[]{:S(2)}, u32[]{:S(2)}) %collective-permute-start.3) | collective-permute-done | bytes 524320 | tf_op jit(solution)/shard_map/ppermute | solution.py:21
  105.9 0.5 broadcast_in_dim.3
  106.5 26.5 %collective-permute-done.4 = bf16[128,2048]{1,0:T(8,128)(2,1)} collective-permute-done((bf16[128,2048]{1,0:T(8,128)(2,1)}, bf16[128,2048]{1,0:T(8,128)(2,1)}, u32[]{:S(2)}, u32[]{:S(2)}) %collective-permute-start.4) | collective-permute-done | bytes 524320 | tf_op jit(solution)/shard_map/ppermute | solution.py:21
  133.3 17.0 %collective-permute-done.5 = bf16[128,2048]{1,0:T(8,128)(2,1)S(1)} collective-permute-done((bf16[128,2048]{1,0:T(8,128)(2,1)}, bf16[128,2048]{1,0:T(8,128)(2,1)S(1)}, u32[]{:S(2)}, u32[]{:S(2)}) %collective-permute-start.5) | collective-permute-done | bytes 524320 | tf_op jit(solution)/shard_map/ppermute | solution.py:21
  150.3 1.1 constant_dynamic-update-slice_fusion.3
  151.4 1.1 constant_dynamic-update-slice_fusion.2
  152.5 18.4 %collective-permute-done.6 = bf16[128,2048]{1,0:T(8,128)(2,1)S(1)} collective-permute-done((bf16[128,2048]{1,0:T(8,128)(2,1)S(1)}, bf16[128,2048]{1,0:T(8,128)(2,1)S(1)}, u32[]{:S(2)}, u32[]{:S(2)}) %collective-permute-start.6) | collective-permute-done | bytes 524320 | tf_op jit(solution)/shard_map/ppermute | solution.py:21
  171.0 2.4 fusion
  173.4 0.7 copy-done.8
  174.1 5.6 %convolution_bitcast_fusion = f32[2048,1024]{0,1:T(8,128)} fusion(bf16[512,1024]{1,0:T(8,128)(2,1)S(1)} %fusion, bf16[512,2048]{1,0:T(8,128)(2,1)S(1)} %copy-done.8), kind=kOutput, calls=%fused_computation | convolution fusion | flops 2147483648 | bytes 11534336 | tf_op jit(solution)/shard_map/dot_general | solution.py:35
  179.9 5.3 %convolution_convert_fusion.2 = bf16[512,1024]{1,0:T(8,128)(2,1)S(1)} fusion(bf16[512,2048]{1,0:T(8,128)(2,1)} %all-gather.3.cloned.1.call-done, bf16[2048,1024]{1,0:T(8,128)(2,1)} %all-gather.5.cloned.1.call-done), kind=kOutput, calls=%fused_computation.8 | convolution fusion | flops 2148007936 | bytes 7340032 | tf_op jit(solution)/shard_map/dot_general | solution.py:52
  185.2 1.0 copy-done.10
  186.2 3.7 convolution_convert_fusion.1
  190.1 6.0 %convolution_convert_fusion = bf16[512,2048]{1,0:T(8,128)(2,1)} fusion(bf16[512,1024]{1,0:T(8,128)(2,1)S(1)} %fusion, bf16[2048,1024]{1,0:T(8,128)(2,1)} %all-gather.5.cloned.1.call-done), kind=kOutput, calls=%fused_computation.1 | convolution fusion | flops 2148532224 | bytes 7340032 | tf_op jit(solution)/shard_map/dot_general | solution.py:29
  196.1 1.6 copy.14
  197.7 101.2 %reduce-scatter.11.cloned.1.call-done = f32[128,2048]{1,0:T(8,128)} async-done(((f32[1024,2048]{1,0:T(8,128)}), f32[128,2048]{1,0:T(8,128)}) %reduce-scatter.11.cloned.1.call-update) | async-done | bytes 1048592 | tf_op jit(solution)/shard_map/reduce_scatter | solution.py:80
  298.9 2.6 multiply_add_fusion
  301.5 147.8 %reduce-scatter.9.cloned.1.call-done = f32[256,1024]{0,1:T(8,128)} async-done(((f32[2048,1024]{0,1:T(8,128)}), f32[256,1024]{0,1:T(8,128)}) %reduce-scatter.9.cloned.1.call-update) | async-done | bytes 1048592 | tf_op jit(solution)/shard_map/reduce_scatter | solution.py:75
  449.4 2.4 multiply_add_fusion.1
  451.8 2.5 copy.15
  454.3 28.3 %reduce-scatter.5.cloned.1.call-done = bf16[128,2048]{1,0:T(8,128)(2,1)} async-done(((bf16[512,2048]{1,0:T(8,128)(2,1)}), bf16[128,2048]{1,0:T(8,128)(2,1)}) %reduce-scatter.5.cloned.1.call-update) | async-done | bytes 524304 | tf_op jit(solution)/shard_map/reduce_scatter | solution.py:58
  482.6 34.2 %reduce-scatter.7.cloned.1.call-done = bf16[128,2048]{1,0:T(8,128)(2,1)} async-done(((bf16[512,2048]{1,0:T(8,128)(2,1)}), bf16[128,2048]{1,0:T(8,128)(2,1)}) %reduce-scatter.7.cloned.1.call-update) | async-done | bytes 524304 | tf_op jit(solution)/shard_map/reduce_scatter | solution.py:68
  (41 shorter events, 0.9 us)
Async XLA Ops:
  7.2 1.6 copy-start
  7.2 172.6 %all-gather.3.cloned.1.call-start = ((), (), s32[]{:S(2)}) async-start(), calls=%async_computation.4 | async-start | bytes 2621440 | tf_op jit(solution)/shard_map/all_gather | solution.py:43
  7.9 171.9 %all-gather.5.cloned.1.call-start = ((), (), s32[]{:S(2)}) async-start(), calls=%async_computation.5 | async-start | bytes 4718592 | tf_op jit(solution)/shard_map/all_gather | solution.py:49
  8.7 290.2 %reduce-scatter.11.cloned.1.call-start = ((), (), s32[]{:S(2)}) async-start(), calls=%async_computation.9 | async-start | bytes 9437184 | tf_op jit(solution)/shard_map/reduce_scatter | solution.py:80
  15.6 1.0 copy-start.3
  15.7 433.7 %reduce-scatter.9.cloned.1.call-start = ((), (), s32[]{:S(2)}) async-start(), calls=%async_computation.8 | async-start | bytes 9437184 | tf_op jit(solution)/shard_map/reduce_scatter | solution.py:75
  16.7 18.0 %collective-permute-start = (bf16[128,2048]{1,0:T(8,128)(2,1)S(1)}, bf16[128,2048]{1,0:T(8,128)(2,1)S(1)}, u32[]{:S(2)}, u32[]{:S(2)}) collective-permute-start(bf16[128,2048]{1,0:T(8,128)(2,1)S(1)} %copy-done.3), channel_id=1, source_target_pairs={{0,4},{4,8},{8,12},{12,16},{16,20},{20,24},{24,28},{28,0},{1,5},{5... | collective-permute-start | bytes 1572872 | tf_op jit(solution)/shard_map/ppermute | solution.py:21
  34.6 15.9 %collective-permute-start.1 = (bf16[128,2048]{1,0:T(8,128)(2,1)S(1)}, bf16[128,2048]{1,0:T(8,128)(2,1)S(1)}, u32[]{:S(2)}, u32[]{:S(2)}) collective-permute-start(bf16[128,2048]{1,0:T(8,128)(2,1)S(1)} %collective-permute-done), channel_id=1, source_target_pairs={{0,4},{4,8},{8,12},{12,16},{16,20},{20,24},{24,28},{28,0},{1,5},{5... | collective-permute-start | bytes 1572872 | tf_op jit(solution)/shard_map/ppermute | solution.py:21
  50.5 0.8 copy-start.4
  51.3 27.6 %collective-permute-start.2 = (bf16[128,2048]{1,0:T(8,128)(2,1)S(1)}, bf16[128,2048]{1,0:T(8,128)(2,1)S(1)}, u32[]{:S(2)}, u32[]{:S(2)}) collective-permute-start(bf16[128,2048]{1,0:T(8,128)(2,1)S(1)} %collective-permute-done.1), channel_id=1, source_target_pairs={{0,4},{4,8},{8,12},{12,16},{16,20},{20,24},{24,28},{28,0},{1,5},{5... | collective-permute-start | bytes 1572872 | tf_op jit(solution)/shard_map/ppermute | solution.py:21
  78.9 0.8 copy-start.6
  79.7 26.2 %collective-permute-start.3 = (bf16[128,2048]{1,0:T(8,128)(2,1)S(1)}, bf16[128,2048]{1,0:T(8,128)(2,1)}, u32[]{:S(2)}, u32[]{:S(2)}) collective-permute-start(bf16[128,2048]{1,0:T(8,128)(2,1)S(1)} %collective-permute-done.2), channel_id=1, source_target_pairs={{0,4},{4,8},{8,12},{12,16},{16,20},{20,24},{24,28},{28,0},{1,5},{5... | collective-permute-start | bytes 1572872 | tf_op jit(solution)/shard_map/ppermute | solution.py:21
  105.9 27.1 %collective-permute-start.4 = (bf16[128,2048]{1,0:T(8,128)(2,1)}, bf16[128,2048]{1,0:T(8,128)(2,1)}, u32[]{:S(2)}, u32[]{:S(2)}) collective-permute-start(bf16[128,2048]{1,0:T(8,128)(2,1)} %collective-permute-done.3), channel_id=1, source_target_pairs={{0,4},{4,8},{8,12},{12,16},{16,20},{20,24},{24,28},{28,0},{1,5},{5... | collective-permute-start | bytes 1572872 | tf_op jit(solution)/shard_map/ppermute | solution.py:21
  105.9 27.2 %copy-start.5 = (bf16[128,2048]{1,0:T(8,128)(2,1)S(1)}, bf16[128,2048]{1,0:T(8,128)(2,1)}, u32[]{:S(2)}) copy-start(bf16[128,2048]{1,0:T(8,128)(2,1)} %copy-done.4) | copy-start | bytes 1572868
  105.9 27.3 %copy-start.7 = (bf16[128,2048]{1,0:T(8,128)(2,1)S(1)}, bf16[128,2048]{1,0:T(8,128)(2,1)}, u32[]{:S(2)}) copy-start(bf16[128,2048]{1,0:T(8,128)(2,1)} %copy-done.6) | copy-start | bytes 1572868
  106.4 64.5 %copy-start.9 = (bf16[512,1024]{1,0:T(8,128)(2,1)S(1)}, bf16[512,1024]{1,0:T(8,128)(2,1)}, u32[]{:S(2)}) copy-start(bf16[512,1024]{1,0:T(8,128)(2,1)} %param.10) | copy-start | bytes 3145732
  133.1 17.2 %collective-permute-start.5 = (bf16[128,2048]{1,0:T(8,128)(2,1)}, bf16[128,2048]{1,0:T(8,128)(2,1)S(1)}, u32[]{:S(2)}, u32[]{:S(2)}) collective-permute-start(bf16[128,2048]{1,0:T(8,128)(2,1)} %collective-permute-done.4), channel_id=1, source_target_pairs={{0,4},{4,8},{8,12},{12,16},{16,20},{20,24},{24,28},{28,0},{1,5},{5... | collective-permute-start | bytes 1572872 | tf_op jit(solution)/shard_map/ppermute | solution.py:21
  150.3 20.6 %collective-permute-start.6 = (bf16[128,2048]{1,0:T(8,128)(2,1)S(1)}, bf16[128,2048]{1,0:T(8,128)(2,1)S(1)}, u32[]{:S(2)}, u32[]{:S(2)}) collective-permute-start(bf16[128,2048]{1,0:T(8,128)(2,1)S(1)} %collective-permute-done.5), channel_id=1, source_target_pairs={{0,4},{4,8},{8,12},{12,16},{16,20},{20,24},{24,28},{28,0},{1,5},{5... | collective-permute-start | bytes 1572872 | tf_op jit(solution)/shard_map/ppermute | solution.py:21
  171.0 2.4 copy-start.1
  171.0 3.1 copy-start.8
  179.7 302.8 %reduce-scatter.5.cloned.1.call-start = ((), (), s32[]{:S(2)}) async-start(), calls=%async_computation.6 | async-start | bytes 2621440 | tf_op jit(solution)/shard_map/reduce_scatter | solution.py:58
  179.8 6.3 %copy-start.2 = (bf16[1024,2048]{1,0:T(8,128)(2,1)S(1)}, bf16[1024,2048]{1,0:T(8,128)(2,1)}, u32[]{:S(2)}) copy-start(bf16[1024,2048]{1,0:T(8,128)(2,1)} %copy-done.1) | copy-start | bytes 12582916
  185.2 1.0 copy-start.10
  189.9 326.8 %reduce-scatter.7.cloned.1.call-start = ((), (), s32[]{:S(2)}) async-start(), calls=%async_computation.7 | async-start | bytes 2621440 | tf_op jit(solution)/shard_map/reduce_scatter | solution.py:68
Sparse Core Ops, SparseCore 0:
  9.5 25.2 all-gather.2
  37.0 101.0 all-gather.4
  141.7 157.1 reduce-scatter.10
  302.4 146.9 reduce-scatter.8
  452.3 30.2 reduce-scatter.4
  485.5 31.1 reduce-scatter.6
